TPU v7x, 256 devices: a whole 4x4x8 slice. The times are simulated.
256 devices in a mesh: ra: 32 (over z, y), cb: 4 (over x), dp: 2 (over core).
Axes of the slice: x: 4, y: 4, z: 8, core: 2. Of those that a mesh axis runs over, the one named last changes fastest.
Arguments:
- stream: bfloat16 [3072, 4096], P(('cb', 'dp'), 'ra'), may hold values from -20 to 20
- up_first: bfloat16 [4096, 16384], P('cb', 'ra'), may hold values from -0.09375 to 0.09375
- down_first: bfloat16 [16384, 4096], P('ra', 'cb'), may hold values from -0.046875 to 0.046875
- up_second: bfloat16 [4096, 16384], P('cb', 'ra'), may hold values from -0.09375 to 0.09375
- down_second: bfloat16 [16384, 4096], P('ra', 'cb'), may hold values from -0.046875 to 0.046875
- gain_first: float32 [4096], P('ra'), may hold values from 0.1 to 1.9
- bias_first: float32 [4096], P('ra'), may hold values from -3 to 3
- gain_second: float32 [4096], P('ra'), may hold values from 0.1 to 1.9
- bias_second: float32 [4096], P('ra'), may hold values from -3 to 3
Outputs:
- result: bfloat16 [3072, 4096], P(('cb', 'dp'), 'ra')
All inputs are finite; a program needn't handle non-finite values.
Results may differ from a plain program's by a relative error of at most 0.0093.
Values may be sent and summed in bfloat16 or wider, within the bound.
No kernel may reach another device: no remote copies, remote signals or barrier semaphores. Data moves between devices by JAX's collectives and lax.ppermute only.
A program may use at most 64 MiB of HBM per device.

v0:
```python
import jax
import jax.numpy as jnp
from jax import lax
from jax.sharding import Mesh
from jax.sharding import PartitionSpec as P

RA = ("ra_0", "ra_1")
RESID = 1.4142135
EPS = 0.5


def whole_of(shard, axes, dim):
    for axis in reversed(axes):
        shard = lax.all_gather(shard, axis, axis=dim, tiled=True)
    return shard


def cut_along(shard, dim, length):
    lengths = shard.shape
    blocks = shard.reshape(*lengths[:dim], length, lengths[dim] // length, *lengths[dim + 1 :])
    return jnp.moveaxis(blocks, dim, 0)


def summed_on_arrival(shard, axis, dim):
    length = lax.axis_size(axis)
    blocks = lax.all_to_all(cut_along(shard, dim, length), axis, 0, 0, tiled=True)
    return jnp.sum(blocks.astype(jnp.float32), axis=0)


def copy_for_each(shard, axis):
    length = lax.axis_size(axis)
    return lax.all_to_all(
        jnp.broadcast_to(shard[None], (length, *shard.shape)), axis, 0, 0, tiled=True
    )


def over_copies(shard, axis):
    everything = copy_for_each(shard, axis)
    return jnp.sum(everything, axis=0)


def in_one(arrays, axis):
    ravelled, at, done = (jnp.concatenate([a.reshape(-1) for a in arrays]), 0, [])
    subtotal = over_copies(ravelled, axis)
    for a in arrays:
        done.append(subtotal[at : at + a.size].reshape(a.shape))
        at += a.size
    return tuple(done)


def sublayer(x, up, down, gain, bias):
    whole = whole_of(x, RA, 1)
    pre = jnp.dot(
        whole, lax.all_gather(up, "cb", axis=0, tiled=True), preferred_element_type=jnp.float32
    )
    hidden = jnp.square(jax.nn.relu(pre)).astype(jnp.bfloat16)
    partial_sums = jnp.dot(
        hidden, lax.all_gather(down, "cb", axis=1, tiled=True), preferred_element_type=jnp.float32
    )
    branch = summed_on_arrival(partial_sums.astype(jnp.bfloat16), RA, 1)
    mixed = RESID * x.astype(jnp.float32) + branch
    width = mixed.shape[1] * lax.axis_size(RA)
    total, squares = in_one(
        (jnp.sum(mixed, axis=1, keepdims=True), jnp.sum(mixed * mixed, axis=1, keepdims=True)), RA
    )
    mean = total / width
    var = squares / width - mean * mean
    centered = mixed - mean
    return (centered * lax.rsqrt(var + EPS) * gain + bias).astype(jnp.bfloat16)


def body(
    stream,
    up_first,
    down_first,
    up_second,
    down_second,
    gain_first,
    bias_first,
    gain_second,
    bias_second,
):
    x = stream
    for up, down, gain, bias in (
        (up_first, down_first, gain_first, bias_first),
        (up_second, down_second, gain_second, bias_second),
    ):
        x = sublayer(x, up, down, gain, bias)
    return x


def solution(mesh):
    torus = Mesh(
        mesh.devices.reshape(8, 4, mesh.shape["cb"], mesh.shape["dp"]), ("ra_0", "ra_1", "cb", "dp")
    )
    in_specs = (
        P(("cb", "dp"), RA),
        P("cb", RA),
        P(RA, "cb"),
        P("cb", RA),
        P(RA, "cb"),
        P(RA),
        P(RA),
        P(RA),
        P(RA),
    )
    out_specs = P(("cb", "dp"), RA)
    return jax.shard_map(body, mesh=torus, in_specs=in_specs, out_specs=out_specs, check_vma=False)
```

profile of v0, /device:TPU:2, one launch (start us, length us, event | category | flops | bytes accessed | tf_op | source)
XLA Modules:
  0.0 448.1 jit_solution(4265126801284976559)
XLA Ops:
  6.5 13.8 %all_gather.24 = bf16[384,512]{1,0:T(8,128)(2,1)} all-gather(bf16[384,128]{1,0:T(8,128)(2,1)} %param.9), channel_id=1, replica_groups=mesh['ra_0'=8,'ra_1'=4,'cb'=4,'dp'=2] {'ra_1'}, dimensions={1}, use_global_device_ids=true | all-gather | bytes 491520 | tf_op jit(solution)/shard_map/all_gather | solution.py:14
  20.5 0.7 all-gather.11.cloned.1.call-update
  21.2 0.7 all-gather.9.cloned.1.call-update
  21.9 0.5 all-gather.15.cloned.1.call-update
  22.5 46.4 %all-gather.7.cloned.1.call-done = bf16[384,4096]{1,0:T(8,128)(2,1)} async-done(((bf16[384,512]{1,0:T(8,128)(2,1)}), bf16[384,4096]{1,0:T(8,128)(2,1)}) %all-gather.7.cloned.1.call-update) | async-done | bytes 3145744 | tf_op jit(solution)/shard_map/all_gather | solution.py:14
  68.9 50.6 %all-gather.11.cloned.1.call-done = bf16[512,4096]{1,0:T(8,128)(2,1)} async-done(((bf16[512,1024]{1,0:T(8,128)(2,1)}), bf16[512,4096]{1,0:T(8,128)(2,1)}) %all-gather.11.cloned.1.call-update) | async-done | bytes 4194320 | tf_op jit(solution)/shard_map/all_gather | solution.py:58
  119.4 53.0 %all-gather.9.cloned.1.call-done = bf16[4096,512]{1,0:T(8,128)(2,1)} async-done(((bf16[1024,512]{1,0:T(8,128)(2,1)}), bf16[4096,512]{1,0:T(8,128)(2,1)}) %all-gather.9.cloned.1.call-update) | async-done | bytes 4194320 | tf_op jit(solution)/shard_map/all_gather | solution.py:54
  172.4 7.8 %fusion = bf16[48,32,8,128]{3,2,1,0:T(8,128)(2,1)S(1)} fusion(bf16[512,4096]{1,0:T(8,128)(2,1)} %all-gather.11.cloned.1.call-done, bf16[384,4096]{1,0:T(8,128)(2,1)} %all-gather.7.cloned.1.call-done, bf16[4096,512]{1,0:T(8,128)(2,1)} %all-gather.9.cloned.1.call-done), kind=kOutput, calls=%fused_computation.6 | convolution fusion | flops 3223388160 | bytes 14680064 | tf_op jit(solution)/shard_map/dot_general | solution.py:57
  180.2 2.6 copy.29
  182.8 10.0 %all-to-all-start = ((bf16[32,384,128]{2,1,0:T(8,128)(2,1)}), bf16[32,384,128]{2,1,0:T(8,128)(2,1)S(1)}, u32[]{:S(2)}, u32[]{:S(2)}) async-start(bf16[32,384,128]{2,1,0:T(8,128)(2,1)} %bitcast.22), calls=%async_computation | async-start | bytes 6291456 | tf_op jit(solution)/shard_map/all_to_all | solution.py:26
  192.9 0.5 all-gather.17.cloned.1.call-update
  193.5 71.5 %all-to-all-done = bf16[32,384,128]{2,1,0:T(8,128)(2,1)S(1)} async-done(((bf16[32,384,128]{2,1,0:T(8,128)(2,1)}), bf16[32,384,128]{2,1,0:T(8,128)(2,1)S(1)}, u32[]{:S(2)}, u32[]{:S(2)}) %all-to-all-start) | async-done | bytes 3145760 | tf_op jit(solution)/shard_map/all_to_all | solution.py:26
  264.9 0.4 convert_reduce_fusion.1
  265.4 0.2 fusion.8
  265.6 16.4 %all_to_all.22 = f32[32,1,768]{2,1,0:T(1,128)S(1)} all-to-all(f32[32,1,768]{2,1,0:T(1,128)S(1)} %broadcast_in_dim.4), channel_id=1, replica_groups=mesh['ra_0'=8,'ra_1'=4,'cb'=4,'dp'=2] {'ra_0','ra_1'}, dimensions={0} | all-to-all | bytes 196608 | tf_op jit(solution)/shard_map/all_to_all | solution.py:32
  282.3 12.7 %all_gather.28 = bf16[384,512]{1,0:T(8,128)(2,1)} all-gather(bf16[384,128]{1,0:T(8,128)(2,1)S(1)} %add_convert_fusion.1), channel_id=1, replica_groups=mesh['ra_0'=8,'ra_1'=4,'cb'=4,'dp'=2] {'ra_1'}, dimensions={1}, use_global_device_ids=true | all-gather | bytes 491520 | tf_op jit(solution)/shard_map/all_gather | solution.py:14
  295.1 40.6 %all-gather.13.cloned.1.call-done = bf16[384,4096]{1,0:T(8,128)(2,1)} async-done(((bf16[384,512]{1,0:T(8,128)(2,1)}), bf16[384,4096]{1,0:T(8,128)(2,1)}) %all-gather.13.cloned.1.call-update) | async-done | bytes 3145744 | tf_op jit(solution)/shard_map/all_gather | solution.py:14
  335.7 7.8 %fusion.1 = bf16[48,32,8,128]{3,2,1,0:T(8,128)(2,1)S(1)} fusion(bf16[512,4096]{1,0:T(8,128)(2,1)} %all-gather.17.cloned.1.call-done, bf16[384,4096]{1,0:T(8,128)(2,1)} %all-gather.13.cloned.1.call-done, bf16[4096,512]{1,0:T(8,128)(2,1)} %all-gather.15.cloned.1.call-done), kind=kOutput, calls=%fused_computation.7 | convolution fusion | flops 3223388160 | bytes 14680064 | tf_op jit(solution)/shard_map/dot_general | solution.py:57
  343.5 0.9 copy.28
  344.4 79.6 %all_to_all.23 = bf16[32,384,128]{2,1,0:T(8,128)(2,1)S(1)} all-to-all(bf16[32,384,128]{2,1,0:T(8,128)(2,1)S(1)} %bitcast.23), channel_id=1, replica_groups=mesh['ra_0'=8,'ra_1'=4,'cb'=4,'dp'=2] {'ra_0','ra_1'}, dimensions={0} | all-to-all | bytes 6291456 | tf_op jit(solution)/shard_map/all_to_all | solution.py:26
  424.1 0.4 convert_reduce_fusion
  424.5 0.2 fusion.9
  424.8 15.6 %all_to_all.24 = f32[32,1,768]{2,1,0:T(1,128)S(1)} all-to-all(f32[32,1,768]{2,1,0:T(1,128)S(1)} %broadcast_in_dim.5), channel_id=1, replica_groups=mesh['ra_0'=8,'ra_1'=4,'cb'=4,'dp'=2] {'ra_0','ra_1'}, dimensions={0} | all-to-all | bytes 196608 | tf_op jit(solution)/shard_map/all_to_all | solution.py:32
  440.5 0.8 add_convert_fusion
  (29 shorter events, 0.8 us)
Async XLA Ops:
  6.5 62.3 %all-gather.7.cloned.1.call-start = ((), (), s32[]{:S(2)}) async-start(), calls=%async_computation.4 | async-start | bytes 3538944 | tf_op jit(solution)/shard_map/all_gather | solution.py:14
  20.4 99.0 %all-gather.11.cloned.1.call-start = ((), (), s32[]{:S(2)}) async-start(), calls=%async_computation.6 | async-start | bytes 5242880 | tf_op jit(solution)/shard_map/all_gather | solution.py:58
  21.2 151.2 %all-gather.9.cloned.1.call-start = ((), (), s32[]{:S(2)}) async-start(), calls=%async_computation.5 | async-start | bytes 5242880 | tf_op jit(solution)/shard_map/all_gather | solution.py:54
  21.9 273.1 %all-gather.15.cloned.1.call-start = ((), (), s32[]{:S(2)}) async-start(), calls=%async_computation.8 | async-start | bytes 5242880 | tf_op jit(solution)/shard_map/all_gather | solution.py:54
  182.8 82.5 %copy-start = (bf16[384,128]{1,0:T(8,128)(2,1)S(1)}, bf16[384,128]{1,0:T(8,128)(2,1)}, u32[]{:S(2)}) copy-start(bf16[384,128]{1,0:T(8,128)(2,1)} %param.9) | copy-start | bytes 294916
  182.8 99.3 %copy-start.1 = (f32[128]{0:T(128)S(1)}, f32[128]{0:T(128)}, u32[]{:S(2)}) copy-start(f32[128]{0:T(128)} %param.15) | copy-start | bytes 1540
  182.8 99.3 %copy-start.2 = (f32[128]{0:T(128)S(1)}, f32[128]{0:T(128)}, u32[]{:S(2)}) copy-start(f32[128]{0:T(128)} %param.14) | copy-start | bytes 1540
  182.8 82.1 %all-to-all-start = ((bf16[32,384,128]{2,1,0:T(8,128)(2,1)}), bf16[32,384,128]{2,1,0:T(8,128)(2,1)S(1)}, u32[]{:S(2)}, u32[]{:S(2)}) async-start(bf16[32,384,128]{2,1,0:T(8,128)(2,1)} %bitcast.22), calls=%async_computation | async-start | bytes 6291456 | tf_op jit(solution)/shard_map/all_to_all | solution.py:26
  192.8 102.2 %all-gather.17.cloned.1.call-start = ((), (), s32[]{:S(2)}) async-start(), calls=%async_computation.9 | async-start | bytes 5242880 | tf_op jit(solution)/shard_map/all_gather | solution.py:58
  193.4 142.3 %all-gather.13.cloned.1.call-start = ((), (), s32[]{:S(2)}) async-start(), calls=%async_computation.7 | async-start | bytes 3538944 | tf_op jit(solution)/shard_map/all_gather | solution.py:14
  344.4 96.0 %copy-start.3 = (f32[128]{0:T(128)S(1)}, f32[128]{0:T(128)}, u32[]{:S(2)}) copy-start(f32[128]{0:T(128)} %param.17) | copy-start | bytes 1540
  344.4 96.0 %copy-start.4 = (f32[128]{0:T(128)S(1)}, f32[128]{0:T(128)}, u32[]{:S(2)}) copy-start(f32[128]{0:T(128)} %param.16) | copy-start | bytes 1540
Sparse Core Ops, SparseCore 0:
  20.5 48.2 all-gather.6
  70.7 48.7 all-gather.10
  121.2 51.0 all-gather.8
  174.0 51.0 all-gather.14
  226.8 51.0 all-gather.16
  295.1 40.5 all-gather.12
where the time goes:
time: 448 us
  waiting for transfers between devices  265 us (59%)
  blocking collectives  138 us (31%)
  matrix products  15.7 us (4%)
  between operations  13.6 us (3%)
  starting transfers between devices  10.2 us (2%)
    all_gather x2, waiting for transfers between devices, whole_of(): shard = lax.all_gather(shard, axis, axis=dim, tiled=True)  87 us
    all_to_all x1, blocking collectives, summed_on_arrival(): lax.all_to_all(cut_along(shard, dim, length), axis, 0, 0, tiled=True)  79.6 us
    all_to_all x1, waiting for transfers between devices, summed_on_arrival(): lax.all_to_all(cut_along(shard, dim, length), axis, 0, 0, tiled=True)  71.5 us
    all_gather x2, waiting for transfers between devices, sublayer(): lax.all_gather(up, 'cb', axis=0, tiled=True)  53 us
    all_gather x2, waiting for transfers between devices, sublayer(): lax.all_gather(down, 'cb', axis=1, tiled=True)  50.6 us
    all_to_all x2, blocking collectives, copy_for_each(): lax.all_to_all(jnp.broadcast_to(shard[None], (length, *shard.shape)), axi...  31.9 us
    all_gather x2, blocking collectives, whole_of(): shard = lax.all_gather(shard, axis, axis=dim, tiled=True)  26.5 us
    dot_general x2, matrix products, sublayer(): jnp.dot(hidden, lax.all_gather(down, 'cb', axis=1, tiled=True), preferred...  15.7 us
  transfers between devices with their start and end apart: 7, of which 5 were waited for; matrix products, arithmetic and copies ran while one was open for 3% of the time, Pallas kernels for 0%

commit v1 on v0

--- a/solution.py
+++ b/solution.py
@@ -7,6 +7,19 @@
 RA = ("ra_0", "ra_1")
 RESID = 1.4142135
 EPS = 0.5
+
+
+def gather_around(x, axis, dim):
+    ways = lax.axis_size(axis)
+    up = [(d, (d + 1) % ways) for d in range(ways)]
+    down = [(d, (d - 1) % ways) for d in range(ways)]
+    earlier, later = ([x], [x])
+    for _ in range(ways // 2):
+        earlier.append(lax.ppermute(earlier[-1], axis, up))
+    for _ in range((ways - 1) // 2):
+        later.append(lax.ppermute(later[-1], axis, down))
+    line = jnp.concatenate([*earlier[::-1], *later[1:]], axis=dim)
+    return jnp.roll(line, (lax.axis_index(axis) - ways // 2) * x.shape[dim], axis=dim)
 
 
 def whole_of(shard, axes, dim):
@@ -54,9 +67,7 @@
         whole, lax.all_gather(up, "cb", axis=0, tiled=True), preferred_element_type=jnp.float32
     )
     hidden = jnp.square(jax.nn.relu(pre)).astype(jnp.bfloat16)
-    partial_sums = jnp.dot(
-        hidden, lax.all_gather(down, "cb", axis=1, tiled=True), preferred_element_type=jnp.float32
-    )
+    partial_sums = jnp.dot(hidden, gather_around(down, "cb", 1), preferred_element_type=jnp.float32)
     branch = summed_on_arrival(partial_sums.astype(jnp.bfloat16), RA, 1)
     mixed = RESID * x.astype(jnp.float32) + branch
     width = mixed.shape[1] * lax.axis_size(RA)

time: 448 us -> 406 us (0.906)
  waiting for transfers between devices: 265 us -> 205 us
  matrix products: 15.7 us -> 26.1 us
  starting transfers between devices: 10.2 us -> 17.6 us
    all_gather x2, waiting for transfers between devices: 87 us -> 1.23 us  [whole_of(): shard = lax.all_gather(shard, axis, axis=dim, tiled=True)]
    ppermute x0 -> x6, waiting for transfers between devices: none -> 80.9 us  [the longest x4 80.9 us: gather_around(): earlier.append(lax.ppermute(earlier[-1], axis, up))]
    all_gather x2 -> x0, waiting for transfers between devices: 50.6 us -> none  [sublayer(): lax.all_gather(down, 'cb', axis=1, tiled=True)]
    dot_general x2, matrix products: 15.7 us -> 26.1 us  [sublayer(): jnp.dot(hidden, gather_around(down, 'cb', 1), preferred_element_type=jnp....]
    ppermute x0 -> x6, starting transfers between devices: none -> 7.49 us  [the longest x4 6.07 us: gather_around(): earlier.append(lax.ppermute(earlier[-1], axis, up))]
  transfers between devices with their start and end apart: 7 -> 11, of which waited for: 5 -> 7; matrix products, arithmetic and copies ran while one was open for 3% -> 0% of each run, Pallas kernels for 0% -> 0%
where the time goes in v1:
time: 406 us; the launch traced here: 405 us
  waiting for transfers between devices  205 us (50%)
  blocking collectives  136 us (33%)
  matrix products  26.1 us (6%)
  starting transfers between devices  17.6 us (4%)
  between operations  13.3 us (3%)
  local copies, waits for them, and re-layouts  4.6 us (1%)
    ppermute x4, waiting for transfers between devices, gather_around(): earlier.append(lax.ppermute(earlier[-1], axis, up))  80.9 us
    all_to_all x1, blocking collectives, summed_on_arrival(): lax.all_to_all(cut_along(shard, dim, length), axis, 0, 0, tiled=True)  77.2 us
    all_to_all x1, waiting for transfers between devices, summed_on_arrival(): lax.all_to_all(cut_along(shard, dim, length), axis, 0, 0, tiled=True)  71.3 us
    all_gather x2, waiting for transfers between devices, sublayer(): lax.all_gather(up, 'cb', axis=0, tiled=True)  50.6 us
    all_to_all x2, blocking collectives, copy_for_each(): lax.all_to_all(jnp.broadcast_to(shard[None], (length, *shard.shape)), axi...  32.1 us
    all_gather x2, blocking collectives, whole_of(): shard = lax.all_gather(shard, axis, axis=dim, tiled=True)  26.5 us
    dot_general x2, matrix products, sublayer(): jnp.dot(hidden, gather_around(down, 'cb', 1), preferred_element_type=jnp....  26.1 us
    all_to_all x1, starting transfers between devices, summed_on_arrival(): lax.all_to_all(cut_along(shard, dim, length), axis, 0, 0, tiled=True)  9.98 us
  transfers between devices with their start and end apart: 11, of which 7 were waited for; matrix products, arithmetic and copies ran while one was open for 0% of the time, Pallas kernels for 0%

profile of v1, /device:TPU:2, one launch (start us, length us, event | category | flops | bytes accessed | tf_op | source)
XLA Modules:
  0.0 405.4 jit_solution(14268393200346028312)
XLA Ops:
  6.5 13.8 %all_gather.18 = bf16[384,512]{1,0:T(8,128)(2,1)} all-gather(bf16[384,128]{1,0:T(8,128)(2,1)} %param.11), channel_id=1, replica_groups=mesh['ra_0'=8,'ra_1'=4,'cb'=4,'dp'=2] {'ra_1'}, dimensions={1}, use_global_device_ids=true | all-gather | bytes 491520 | tf_op jit(solution)/shard_map/all_gather | solution.py:27
  21.2 1.6 collective-permute-start
  23.3 21.6 %collective-permute-done = bf16[512,1024]{1,0:T(8,128)(2,1)S(1)} collective-permute-done((bf16[512,1024]{1,0:T(8,128)(2,1)}, bf16[512,1024]{1,0:T(8,128)(2,1)S(1)}, u32[]{:S(2)}, u32[]{:S(2)}) %collective-permute-start) | collective-permute-done | bytes 1048608 | tf_op jit(solution)/shard_map/ppermute | solution.py:18
  44.9 1.5 collective-permute-start.1
  46.4 21.2 %collective-permute-done.1 = bf16[512,1024]{1,0:T(8,128)(2,1)S(1)} collective-permute-done((bf16[512,1024]{1,0:T(8,128)(2,1)S(1)}, bf16[512,1024]{1,0:T(8,128)(2,1)S(1)}, u32[]{:S(2)}, u32[]{:S(2)}) %collective-permute-start.1) | collective-permute-done | bytes 1048608 | tf_op jit(solution)/shard_map/ppermute | solution.py:18
  67.6 1.2 all-gather.5.cloned.1.call-done
  68.8 50.6 %all-gather.7.cloned.1.call-done = bf16[4096,512]{1,0:T(8,128)(2,1)} async-done(((bf16[1024,512]{1,0:T(8,128)(2,1)}), bf16[4096,512]{1,0:T(8,128)(2,1)}) %all-gather.7.cloned.1.call-update) | async-done | bytes 4194320 | tf_op jit(solution)/shard_map/all_gather | solution.py:67
  119.4 13.1 %fusion.18 = bf16[48,32,8,128]{3,2,1,0:T(8,128)(2,1)S(1)} fusion(s32[]{:T(128)S(6)} %select_n.13, bf16[512,1024]{1,0:T(8,128)(2,1)} %copy-done.7, bf16[512,1024]{1,0:T(8,128)(2,1)} %copy-done.5, bf16[512,1024]{1,0:T(8,128)(2,1)} %param.13, bf16[512,1024]{1,0:T(8,128)(2,1)} %copy-done.6, bf16[384,4096]{1,0:T(8,128)(2,1)} %all-gather.5.cloned.1.call-done, ...), kind=kOutput, calls=%fused_computation.36 | convolution fusion | flops 3256942592 | bytes 14680068 | tf_op jit(solution)/shard_map/dot_general | solution.py:70
  132.5 2.5 copy.29
  135.0 10.0 %all-to-all-start = ((bf16[32,384,128]{2,1,0:T(8,128)(2,1)}), bf16[32,384,128]{2,1,0:T(8,128)(2,1)S(1)}, u32[]{:S(2)}, u32[]{:S(2)}) async-start(bf16[32,384,128]{2,1,0:T(8,128)(2,1)} %bitcast.20), calls=%async_computation | async-start | bytes 6291456 | tf_op jit(solution)/shard_map/all_to_all | solution.py:39
  145.8 71.3 %all-to-all-done = bf16[32,384,128]{2,1,0:T(8,128)(2,1)S(1)} async-done(((bf16[32,384,128]{2,1,0:T(8,128)(2,1)}), bf16[32,384,128]{2,1,0:T(8,128)(2,1)S(1)}, u32[]{:S(2)}, u32[]{:S(2)}) %all-to-all-start) | async-done | bytes 3145760 | tf_op jit(solution)/shard_map/all_to_all | solution.py:39
  217.8 16.4 %all_to_all.22 = f32[32,1,768]{2,1,0:T(1,128)S(1)} all-to-all(f32[32,1,768]{2,1,0:T(1,128)S(1)} %broadcast_in_dim.4), channel_id=1, replica_groups=mesh['ra_0'=8,'ra_1'=4,'cb'=4,'dp'=2] {'ra_0','ra_1'}, dimensions={0} | all-to-all | bytes 196608 | tf_op jit(solution)/shard_map/all_to_all | solution.py:45
  234.5 12.7 %all_gather.21 = bf16[384,512]{1,0:T(8,128)(2,1)} all-gather(bf16[384,128]{1,0:T(8,128)(2,1)S(1)} %add_convert_fusion.1), channel_id=1, replica_groups=mesh['ra_0'=8,'ra_1'=4,'cb'=4,'dp'=2] {'ra_1'}, dimensions={1}, use_global_device_ids=true | all-gather | bytes 491520 | tf_op jit(solution)/shard_map/all_gather | solution.py:27
  247.2 1.2 collective-permute-start.3
  248.4 0.9 collective-permute-start.5
  249.3 19.7 %collective-permute-done.3 = bf16[512,1024]{1,0:T(8,128)(2,1)S(1)} collective-permute-done((bf16[512,1024]{1,0:T(8,128)(2,1)}, bf16[512,1024]{1,0:T(8,128)(2,1)S(1)}, u32[]{:S(2)}, u32[]{:S(2)}) %collective-permute-start.3) | collective-permute-done | bytes 1048608 | tf_op jit(solution)/shard_map/ppermute | solution.py:18
  269.0 1.1 copy-done.8
  270.1 1.8 collective-permute-start.4
  271.9 18.4 %collective-permute-done.4 = bf16[512,1024]{1,0:T(8,128)(2,1)} collective-permute-done((bf16[512,1024]{1,0:T(8,128)(2,1)S(1)}, bf16[512,1024]{1,0:T(8,128)(2,1)}, u32[]{:S(2)}, u32[]{:S(2)}) %collective-permute-start.4) | collective-permute-done | bytes 1048608 | tf_op jit(solution)/shard_map/ppermute | solution.py:18
  290.3 13.1 %fusion.21 = bf16[48,32,8,128]{3,2,1,0:T(8,128)(2,1)S(1)} fusion(s32[]{:T(128)S(6)} %select_n.13, bf16[512,1024]{1,0:T(8,128)(2,1)} %collective-permute-done.4, bf16[512,1024]{1,0:T(8,128)(2,1)} %copy-done.8, bf16[512,1024]{1,0:T(8,128)(2,1)} %param.15, bf16[512,1024]{1,0:T(8,128)(2,1)} %collective-permute-done.5, ...), kind=kOutput, calls=%fused_computation.37 | convolution fusion | flops 3256942592 | bytes 14680068 | tf_op jit(solution)/shard_map/dot_general | solution.py:70
  303.4 0.9 copy.28
  304.2 77.2 %all_to_all.23 = bf16[32,384,128]{2,1,0:T(8,128)(2,1)S(1)} all-to-all(bf16[32,384,128]{2,1,0:T(8,128)(2,1)S(1)} %bitcast.21), channel_id=1, replica_groups=mesh['ra_0'=8,'ra_1'=4,'cb'=4,'dp'=2] {'ra_0','ra_1'}, dimensions={0} | all-to-all | bytes 6291456 | tf_op jit(solution)/shard_map/all_to_all | solution.py:39
  382.2 15.7 %all_to_all.24 = f32[32,1,768]{2,1,0:T(1,128)S(1)} all-to-all(f32[32,1,768]{2,1,0:T(1,128)S(1)} %broadcast_in_dim.5), channel_id=1, replica_groups=mesh['ra_0'=8,'ra_1'=4,'cb'=4,'dp'=2] {'ra_0','ra_1'}, dimensions={0} | all-to-all | bytes 196608 | tf_op jit(solution)/shard_map/all_to_all | solution.py:45
  398.0 0.8 add_convert_fusion
  (43 shorter events, 3.8 us)
Async XLA Ops:
  6.5 62.3 %all-gather.5.cloned.1.call-start = ((), (), s32[]{:S(2)}) async-start(), calls=%async_computation.4 | async-start | bytes 3538944 | tf_op jit(solution)/shard_map/all_gather | solution.py:27
  20.4 99.0 %all-gather.7.cloned.1.call-start = ((), (), s32[]{:S(2)}) async-start(), calls=%async_computation.5 | async-start | bytes 5242880 | tf_op jit(solution)/shard_map/all_gather | solution.py:67
  21.2 23.7 %collective-permute-start = (bf16[512,1024]{1,0:T(8,128)(2,1)}, bf16[512,1024]{1,0:T(8,128)(2,1)S(1)}, u32[]{:S(2)}, u32[]{:S(2)}) collective-permute-start(bf16[512,1024]{1,0:T(8,128)(2,1)} %param.13), channel_id=1, source_target_pairs={{0,2},{2,4},{4,6},{6,0},{1,3},{3,5},{5,7},{7,1},{8,10},{10,12},{12... | collective-permute-start | bytes 3145736 | tf_op jit(solution)/shard_map/ppermute | solution.py:18
  22.7 23.7 %collective-permute-start.2 = (bf16[512,1024]{1,0:T(8,128)(2,1)}, bf16[512,1024]{1,0:T(8,128)(2,1)S(1)}, u32[]{:S(2)}, u32[]{:S(2)}) collective-permute-start(bf16[512,1024]{1,0:T(8,128)(2,1)} %param.13), channel_id=1, source_target_pairs={{0,6},{2,0},{4,2},{6,4},{1,7},{3,1},{5,3},{7,5},{8,14},{10,8},{12,... | collective-permute-start | bytes 3145736 | tf_op jit(solution)/shard_map/ppermute | solution.py:20
  44.9 23.9 %copy-start.5 = (bf16[512,1024]{1,0:T(8,128)(2,1)}, bf16[512,1024]{1,0:T(8,128)(2,1)S(1)}, u32[]{:S(2)}) copy-start(bf16[512,1024]{1,0:T(8,128)(2,1)S(1)} %collective-permute-done) | copy-start | bytes 3145732
  44.9 22.7 %collective-permute-start.1 = (bf16[512,1024]{1,0:T(8,128)(2,1)S(1)}, bf16[512,1024]{1,0:T(8,128)(2,1)S(1)}, u32[]{:S(2)}, u32[]{:S(2)}) collective-permute-start(bf16[512,1024]{1,0:T(8,128)(2,1)S(1)} %collective-permute-done), channel_id=1, source_target_pairs={{0,2},{2,4},{4,6},{6,0},{1,3},{3,5},{5,7},{7,1},{8,10},{10,12},{12... | collective-permute-start | bytes 3145736 | tf_op jit(solution)/shard_map/ppermute | solution.py:18
  46.4 22.4 %copy-start.6 = (bf16[512,1024]{1,0:T(8,128)(2,1)}, bf16[512,1024]{1,0:T(8,128)(2,1)S(1)}, u32[]{:S(2)}) copy-start(bf16[512,1024]{1,0:T(8,128)(2,1)S(1)} %collective-permute-done.2) | copy-start | bytes 3145732
  67.6 1.2 copy-start.7
  135.0 82.5 %copy-start = (bf16[384,128]{1,0:T(8,128)(2,1)S(1)}, bf16[384,128]{1,0:T(8,128)(2,1)}, u32[]{:S(2)}) copy-start(bf16[384,128]{1,0:T(8,128)(2,1)} %param.11) | copy-start | bytes 294916
  135.0 99.3 %copy-start.1 = (f32[128]{0:T(128)S(1)}, f32[128]{0:T(128)}, u32[]{:S(2)}) copy-start(f32[128]{0:T(128)} %param.17) | copy-start | bytes 1540
  135.0 99.3 %copy-start.2 = (f32[128]{0:T(128)S(1)}, f32[128]{0:T(128)}, u32[]{:S(2)}) copy-start(f32[128]{0:T(128)} %param.16) | copy-start | bytes 1540
  135.0 82.1 %all-to-all-start = ((bf16[32,384,128]{2,1,0:T(8,128)(2,1)}), bf16[32,384,128]{2,1,0:T(8,128)(2,1)S(1)}, u32[]{:S(2)}, u32[]{:S(2)}) async-start(bf16[32,384,128]{2,1,0:T(8,128)(2,1)} %bitcast.20), calls=%async_computation | async-start | bytes 6291456 | tf_op jit(solution)/shard_map/all_to_all | solution.py:39
  145.0 145.3 %all-gather.11.cloned.1.call-start = ((), (), s32[]{:S(2)}) async-start(), calls=%async_computation.7 | async-start | bytes 5242880 | tf_op jit(solution)/shard_map/all_gather | solution.py:67
  145.7 144.5 %all-gather.9.cloned.1.call-start = ((), (), s32[]{:S(2)}) async-start(), calls=%async_computation.6 | async-start | bytes 3538944 | tf_op jit(solution)/shard_map/all_gather | solution.py:27
  247.2 21.8 %collective-permute-start.3 = (bf16[512,1024]{1,0:T(8,128)(2,1)}, bf16[512,1024]{1,0:T(8,128)(2,1)S(1)}, u32[]{:S(2)}, u32[]{:S(2)}) collective-permute-start(bf16[512,1024]{1,0:T(8,128)(2,1)} %param.15), channel_id=1, source_target_pairs={{0,2},{2,4},{4,6},{6,0},{1,3},{3,5},{5,7},{7,1},{8,10},{10,12},{12... | collective-permute-start | bytes 3145736 | tf_op jit(solution)/shard_map/ppermute | solution.py:18
  248.4 23.4 %collective-permute-start.5 = (bf16[512,1024]{1,0:T(8,128)(2,1)}, bf16[512,1024]{1,0:T(8,128)(2,1)}, u32[]{:S(2)}, u32[]{:S(2)}) collective-permute-start(bf16[512,1024]{1,0:T(8,128)(2,1)} %param.15), channel_id=1, source_target_pairs={{0,6},{2,0},{4,2},{6,4},{1,7},{3,1},{5,3},{7,5},{8,14},{10,8},{12,... | collective-permute-start | bytes 3145736 | tf_op jit(solution)/shard_map/ppermute | solution.py:20
  269.0 1.1 copy-start.8
  270.1 20.2 %collective-permute-start.4 = (bf16[512,1024]{1,0:T(8,128)(2,1)S(1)}, bf16[512,1024]{1,0:T(8,128)(2,1)}, u32[]{:S(2)}, u32[]{:S(2)}) collective-permute-start(bf16[512,1024]{1,0:T(8,128)(2,1)S(1)} %collective-permute-done.3), channel_id=1, source_target_pairs={{0,2},{2,4},{4,6},{6,0},{1,3},{3,5},{5,7},{7,1},{8,10},{10,12},{12... | collective-permute-start | bytes 3145736 | tf_op jit(solution)/shard_map/ppermute | solution.py:18
  304.2 93.8 %copy-start.3 = (f32[128]{0:T(128)S(1)}, f32[128]{0:T(128)}, u32[]{:S(2)}) copy-start(f32[128]{0:T(128)} %param.19) | copy-start | bytes 1540
  304.2 93.8 %copy-start.4 = (f32[128]{0:T(128)S(1)}, f32[128]{0:T(128)}, u32[]{:S(2)}) copy-start(f32[128]{0:T(128)} %param.18) | copy-start | bytes 1540
Sparse Core Ops, SparseCore 0:
  20.5 48.2 all-gather.4
  70.6 48.7 all-gather.6
  147.6 51.0 all-gather.10
  247.3 40.4 all-gather.8
